TPU v7x, 512 devices: a whole 4x8x8 slice. The times are simulated.
512 devices in a mesh: sp: 64 (over z, y), fs: 4 (over x), tp: 2 (over core).
Axes of the slice: x: 4, y: 8, z: 8, core: 2. Of those that a mesh axis runs over, the one named last changes fastest.
Arguments:
- tokens: bfloat16 [4, 8192, 2048], P('fs', ('sp', 'tp')), may hold values from -6 to 6
- input_norm_gain: float32 [2048], replicated, may hold values from 0.1 to 1.9
- pooling_input_weight: bfloat16 [2048, 1024], P('sp', 'tp'), may hold values from -0.125 to 0.125
- query_weight: bfloat16 [2048, 1024], P('sp', 'tp'), may hold values from -0.125 to 0.125
- forget_weight: bfloat16 [2048, 1024], P('sp', 'tp'), may hold values from -0.125 to 0.125
- value_weight: bfloat16 [2048, 1024], P('sp', 'tp'), may hold values from -0.125 to 0.125
- pooling_group_maps: bfloat16 [4, 256, 256], P('tp'), may hold values from -0.375 to 0.375
- pooling_scale: float32 [1024], P('tp'), may hold values from 0.1 to 1.9
- lower_bound_logits: float32 [1024], P('tp')
- decay_spike: float32 [4, 8192, 8], P('fs', 'sp', 'tp'), may hold values from -0.75 to 0
- head_norm_gain: float32 [1024], P('tp'), may hold values from 0.1 to 1.9
- pooling_output_weight: bfloat16 [1024, 2048], P('tp', 'sp'), may hold values from -0.125 to 0.125
- recurrent_output_weight: bfloat16 [1024, 2048], P('tp', 'sp'), may hold values from -0.125 to 0.125
Outputs:
- mixed: bfloat16 [4, 8192, 2048], P('fs', ('sp', 'tp'))
All inputs are finite; a program needn't handle non-finite values.
Results may differ from a plain program's by a relative error of at most 0.013.
Values may be sent and summed in bfloat16 or wider, within the bound.
A program may use at most 64 MiB of HBM per device.

v0:
```python
import jax
import jax.numpy as jnp
from jax import lax
from jax.sharding import Mesh
from jax.sharding import PartitionSpec as P

BLOCK = 64
SP = ("sp_0", "sp_1")
SP_TP = ("sp_0", "sp_1", "tp")
EPSILON = 1e-06
HIGHEST = lax.Precision.HIGHEST


def in_order(tiles, dim):
    tiles = jnp.moveaxis(tiles, 0, dim)
    dims = tiles.shape
    return tiles.reshape(*dims[:dim], dims[dim] * dims[dim + 1], *dims[dim + 2 :])


def all_blocks(shard, axes, sequence):
    tiles = shard
    for k in sequence:
        tiles = lax.all_gather(tiles, axes[k])
    done = sequence[::-1]
    back = [done.index(k) for k in range(len(axes))]
    tiles = tiles.transpose(*back, *range(len(axes), tiles.ndim))
    return tiles.reshape(-1, *shard.shape)


def gathered_by_axis(shard, axes, sequence, dim):
    return in_order(all_blocks(shard, axes, sequence), dim)


def shifted(value, axis, steps):
    count = lax.axis_size(axis)
    first, last = (max(0, -steps), min(count, count - steps))
    return lax.ppermute(value, axis, [(source, source + steps) for source in range(first, last)])


def filled_with(shard, identity):
    return jax.tree.map(
        lambda part, zero: jnp.zeros_like(part) + jnp.asarray(zero, part.dtype), shard, identity
    )


def carried_in(shard, axes, combine, identity):
    before = start = filled_with(shard, identity)
    total = shard
    for axis in reversed(axes):
        peers, here = (lax.axis_size(axis), lax.axis_index(axis))
        pieces = jax.tree.map(
            lambda part, kind: lax.all_gather(part.astype(kind), axis),
            total,
            (jnp.bfloat16, jnp.bfloat16),
        )
        inside, total = (start, start)
        for k in range(peers):
            passed = k < here
            total = combine(
                total, jax.tree.map(lambda part, own: part[k].astype(own.dtype), pieces, shard)
            )
            inside = jax.tree.map(lambda new, old: jnp.where(passed, new, old), total, inside)
        before = combine(inside, before)
    return before


def cut_along(shard, dim, peers):
    before, after = (shard.shape[:dim], shard.shape[dim + 1 :])
    return jnp.moveaxis(shard.reshape(*before, peers, -1, *after), dim, 0)


def summed_on_arrival(shard, axis, dim):
    tiles = cut_along(shard, dim, lax.axis_size(axis))
    arrived = lax.all_to_all(tiles, axis, split_axis=0, concat_axis=0, tiled=True)
    return arrived.astype(jnp.float32).sum(axis=0)


def rms_scale(values, gain):
    return values * lax.rsqrt(jnp.mean(values * values, axis=-1, keepdims=True) + EPSILON) * gain


def join_state(earlier, later):
    decay_one, state_one = earlier
    decay_two, state_two = later
    return (decay_one * decay_two, decay_two[..., None] * state_one + state_two)


def body(
    tokens,
    input_norm_gain,
    pooling_input_weight,
    query_weight,
    forget_weight,
    value_weight,
    pooling_group_maps,
    pooling_scale,
    lower_bound_logits,
    decay_spike,
    head_norm_gain,
    pooling_output_weight,
    recurrent_output_weight,
):
    gathered = lax.all_gather(tokens, "tp", axis=1, tiled=True)[0]
    length_total = gathered.shape[0]
    normed = rms_scale(gathered.astype(jnp.float32), input_norm_gain).astype(jnp.bfloat16)
    pool_width = pooling_input_weight.shape[1]
    rec_width = query_weight.shape[1]
    stacked = jnp.concatenate(
        [pooling_input_weight, query_weight, forget_weight, value_weight], axis=1
    )
    out_local = jnp.concatenate([pooling_output_weight, recurrent_output_weight], axis=0)
    projected = jnp.dot(
        normed, lax.all_gather(stacked, SP, axis=0, tiled=True), preferred_element_type=jnp.float32
    )
    out_full = gathered_by_axis(out_local, SP, (0, 1), 1)
    rounded = lax.optimization_barrier(projected.astype(jnp.bfloat16))
    pool_input = rounded[:, :pool_width]
    query_matrix = rounded[:, pool_width : pool_width + rec_width].astype(jnp.float32)
    forget_gate_logit = rounded[:, pool_width + rec_width : pool_width + 2 * rec_width].astype(
        jnp.float32
    )
    value_projected = rounded[:, pool_width + 2 * rec_width :].astype(jnp.float32)
    groups_local = pooling_group_maps.shape[0]
    group_size = pooling_group_maps.shape[1]
    reach_rows = 2 ** (groups_local * lax.axis_size("tp"))
    previous = shifted(pool_input[length_total - reach_rows :], SP, 1)
    extended = jnp.concatenate([previous, pool_input], axis=0).astype(jnp.float32)
    extended = extended.reshape(reach_rows + length_total, groups_local, group_size)
    group_ids = lax.axis_index("tp") * groups_local + jnp.arange(groups_local, dtype=jnp.int32)
    windows = jnp.left_shift(jnp.int32(2), group_ids)
    window_sum = jnp.zeros((length_total, groups_local, group_size), jnp.float32)
    for offset in range(reach_rows):
        inside = (offset < windows).astype(jnp.float32)
        window_sum = (
            window_sum
            + extended[reach_rows - offset : reach_rows - offset + length_total] * inside[:, None]
        )
    position_index = lax.axis_index(SP) * length_total + jnp.arange(length_total, dtype=jnp.int32)
    counts = jnp.minimum(position_index[:, None] + 1, windows[None, :]).astype(jnp.float32)
    pool_diff = (window_sum / counts[:, :, None] - extended[reach_rows:]).astype(jnp.bfloat16)
    pool_mapped = jnp.einsum(
        "tgc,gcd->tgd", pool_diff, pooling_group_maps, preferred_element_type=jnp.float32
    )
    pool_out = (pool_mapped.reshape(length_total, pool_width) * pooling_scale).astype(jnp.bfloat16)
    local_heads = decay_spike.shape[2]
    head_width = rec_width // local_heads
    blocks = length_total // BLOCK
    block_layout = (blocks, BLOCK, local_heads, head_width)
    reader = jax.nn.silu(query_matrix).reshape(block_layout)
    key_gate_value = jax.nn.sigmoid(-lower_bound_logits) * jax.nn.sigmoid(-forget_gate_logit)
    decay_logarithm = (
        jnp.log1p(-key_gate_value).reshape(length_total, local_heads, head_width)
        + decay_spike[0][:, :, None]
    ).reshape(block_layout)
    key_rows = key_gate_value.reshape(block_layout)
    value_rows = value_projected.reshape(block_layout)
    inner_log = jnp.cumsum(decay_logarithm, axis=1)
    read_scaled = reader * jnp.exp(inner_log)
    key_scaled = key_rows * jnp.exp(-inner_log)
    causal = (jnp.arange(BLOCK)[:, None] >= jnp.arange(BLOCK)[None, :]).astype(jnp.float32)
    scores = jnp.einsum("nthd,nshd->nhts", read_scaled, key_scaled, precision=HIGHEST) * causal
    within = jnp.einsum("nhts,nshe->nthe", scores, value_rows, precision=HIGHEST)
    closing = inner_log[:, -1]
    key_tail = key_rows * jnp.exp(closing[:, None] - inner_log)
    deltas = jnp.einsum("nshd,nshe->nhde", key_tail, value_rows, precision=HIGHEST)
    block_decay = jnp.exp(closing)

    def advance(carried, input_batch):
        decay_now, delta_now = input_batch
        return (decay_now[..., None] * carried + delta_now, carried)

    initial = jnp.zeros((local_heads, head_width, head_width), jnp.float32)
    device_state, entry_states = lax.scan(advance, initial, (block_decay, deltas))
    device_decay = jnp.exp(jnp.sum(closing, axis=0))
    scanned = carried_in(
        (device_decay, device_state),
        SP,
        join_state,
        (jnp.ones_like(device_decay), jnp.zeros_like(device_state)),
    )
    prior_state = scanned[1]
    before = jnp.cumsum(closing, axis=0) - closing
    start_states = entry_states + jnp.exp(before)[..., None] * prior_state[None]
    read_out = within + jnp.einsum("nthd,nhde->nthe", read_scaled, start_states, precision=HIGHEST)
    read_out = read_out.reshape(length_total, local_heads, head_width)
    recurrent_output = (
        rms_scale(read_out, 1.0).reshape(length_total, rec_width) * head_norm_gain
    ).astype(jnp.bfloat16)
    mixed_rows = jnp.concatenate([pool_out, recurrent_output], axis=1)
    summed = summed_on_arrival(
        jnp.dot(mixed_rows, out_full, preferred_element_type=jnp.float32).astype(jnp.bfloat16),
        "tp",
        0,
    )
    return summed.astype(jnp.bfloat16)[None]


def solution(mesh):
    torus = Mesh(
        mesh.devices.reshape(8, 8, mesh.shape["fs"], mesh.shape["tp"]), ("sp_0", "sp_1", "fs", "tp")
    )
    return jax.shard_map(
        body,
        mesh=torus,
        in_specs=(
            P("fs", SP_TP, None),
            P(),
            P(SP, "tp"),
            P(SP, "tp"),
            P(SP, "tp"),
            P(SP, "tp"),
            P("tp", None, None),
            P("tp"),
            P("tp"),
            P("fs", SP, "tp"),
            P("tp"),
            P("tp", SP),
            P("tp", SP),
        ),
        out_specs=P("fs", SP_TP, None),
        check_vma=False,
    )
```

profile of v0, /device:TPU:1, one launch (start us, length us, event | category | flops | bytes accessed | tf_op | source)
XLA Modules:
  0.0 277.8 jit_solution(2328554561795465922)
XLA Ops:
  6.5 0.0 copy-start
  6.5 0.0 all-gather.10.cloned.1.call-start
  6.5 1.5 pad_maximum_fusion
  8.1 0.0 all-gather.10.cloned.1.call-update
  8.1 0.0 all-gather.16.cloned.1.call-start
  8.1 0.8 pad_maximum_fusion.1
  8.9 27.3 %all-gather.2 = bf16[8192,32]{0,1:T(8,128)(2,1)S(1)} all-gather(bf16[1024,32]{0,1:T(8,128)(2,1)S(1)} %pad_maximum_fusion.1), channel_id=4, replica_groups=mesh['sp_0'=8,'sp_1'=8,'fs'=4,'tp'=2] {'sp_0'}, dimensions={0}, use_global_device_ids=true | all-gather | bytes 589824 | tf_op jit(solution)/shard_map/all_gather | solution.py:23
  36.2 1.1 copy.197
  37.4 0.0 all-gather.16.cloned.1.call-update
  37.4 0.0 all-gather.14.cloned.1.call-start
  37.5 0.8 copy.177
  38.3 7.8 %all_gather.36 = bf16[1,128,2048]{2,1,0:T(8,128)(2,1)S(1)} all-gather(bf16[1,64,2048]{2,1,0:T(8,128)(2,1)} %param.15), channel_id=1, replica_groups=mesh['sp_0'=8,'sp_1'=8,'fs'=4,'tp'=2] {'tp'}, dimensions={1}, use_global_device_ids=true | all-gather | bytes 786432 | tf_op jit(solution)/shard_map/all_gather | solution.py:103
  46.2 0.2 fusion.2
  46.4 0.7 add_divide_fusion
  47.0 67.8 %all-gather.10.cloned.1.call-done = bf16[2048,2048]{1,0:T(8,128)(2,1)} async-done(((bf16[32,2048]{1,0:T(8,128)(2,1)}), bf16[2048,2048]{1,0:T(8,128)(2,1)}) %all-gather.10.cloned.1.call-update) | async-done | bytes 8388624 | tf_op jit(solution)/shard_map/all_gather | solution.py:113
  114.9 4.7 %convolution_convert_fusion = bf16[128,2048]{1,0:T(8,128)(2,1)S(1)} fusion(bf16[2048,2048]{1,0:T(8,128)(2,1)} %all-gather.10.cloned.1.call-done, bf16[1,128,2048]{2,1,0:T(8,128)(2,1)S(1)} %all_gather.36, f32[2048]{0:T(1024)} %param.16, f32[128]{0:T(128)S(1)} %add_rsqrt_fusion.1), kind=kOutput, calls=%fused_computation.3 | convolution fusion | flops 1075052544 | bytes 9445888 | tf_op jit(solution)/shard_map/dot_general | solution.py:112
  119.6 0.2 negate_log-plus-one_fusion
  119.8 0.1 reshape.384
  119.9 0.1 reshape.383
  120.0 0.1 reshape.385
  120.2 0.2 fusion.54
  120.4 0.2 exponential_multiply_fusion
  120.6 0.6 fusion.48
  121.2 0.5 while.13
  121.3 0.2 bitcast_add_fusion.2
  121.5 0.2 bitcast_add_fusion.2
  121.7 0.7 convert_element_type.533
  122.4 0.0 all-gather.14.cloned.1.call-update
  122.4 0.0 all-gather.12.cloned.1.call-start
  122.6 0.1 minimum_convert_fusion
  122.7 49.5 %all-gather.16.cloned.1.call-done = bf16[64,1024,32]{1,0,2:T(8,128)(2,1)} async-done(((bf16[8,1024,32]{1,0,2:T(8,128)(2,1)}), bf16[64,1024,32]{1,0,2:T(8,128)(2,1)}) %all-gather.16.cloned.1.call-update) | async-done | bytes 4194320 | tf_op jit(solution)/shard_map/all_gather | solution.py:23
  172.2 6.5 %copy.176 = bf16[8,8,1024,32]{2,3,1,0:T(8,128)(2,1)} copy(bf16[8,8,1024,32]{2,0,1,3:T(8,128)(2,1)} %bitcast.379) | data formatting | bytes 8388608 | tf_op jit(solution)/shard_map/transpose | solution.py:26
  178.7 11.0 %all-gather.4 = bf16[8,4,128]{2,1,0:T(4,128)(2,1)S(1)} all-gather(bf16[1,4,128]{2,1,0:T(4,128)(2,1)S(1)} %fusion.75), channel_id=2, replica_groups=mesh['sp_0'=8,'sp_1'=8,'fs'=4,'tp'=2] {'sp_1'}, dimensions={0}, use_global_device_ids=true | all-gather | bytes 9216 | tf_op jit(solution)/shard_map/all_gather | solution.py:52
  189.6 14.1 %all_gather.39 = bf16[8,4,128]{2,1,0:T(4,128)(2,1)S(1)} all-gather(bf16[1,4,128]{2,1,0:T(4,128)(2,1)S(1)} %fusion.65), channel_id=1, replica_groups=mesh['sp_0'=8,'sp_1'=8,'fs'=4,'tp'=2] {'sp_0'}, dimensions={0}, use_global_device_ids=true | all-gather | bytes 9216 | tf_op jit(solution)/shard_map/all_gather | solution.py:52
  203.8 5.7 %all-gather.14.cloned.1.call-done = bf16[32,128,128]{2,1,0:T(8,128)(2,1)} async-done(((bf16[4,128,128]{2,1,0:T(8,128)(2,1)}), bf16[32,128,128]{2,1,0:T(8,128)(2,1)}) %all-gather.14.cloned.1.call-update) | async-done | bytes 1048592 | tf_op jit(solution)/shard_map/all_gather | solution.py:52
  209.4 2.4 fusion.52
  211.9 0.0 all-gather.12.cloned.1.call-update
  211.9 2.7 collective-permute-start
  214.6 0.5 convolution_multiply_fusion
  215.2 0.3 fusion.62
  215.4 0.0 collective-permute-done
  215.5 0.5 fusion.90
  216.0 0.0 copy-start.2
  216.0 0.0 copy-start.1
  216.0 0.0 copy-done
  216.0 0.5 convolution_bitcast_fusion
  216.5 0.0 copy-start.3
  216.5 0.1 copy.164
  216.7 0.0 copy-done.2
  216.7 0.1 fusion.47
  216.8 36.3 %all-gather.12.cloned.1.call-done = bf16[8,4,128,128]{3,2,1,0:T(8,128)(2,1)} async-done(((bf16[1,4,128,128]{3,2,1,0:T(8,128)(2,1)}), bf16[8,4,128,128]{3,2,1,0:T(8,128)(2,1)}) %all-gather.12.cloned.1.call-update) | async-done | bytes 1048592 | tf_op jit(solution)/shard_map/all_gather | solution.py:52
  253.1 0.0 copy-done.1
  253.1 2.9 %fusion.44 = f32[4,128,128]{2,1,0:T(8,128)S(1)} fusion(bf16[8,4,128,128]{3,2,1,0:T(8,128)(2,1)} %all-gather.12.cloned.1.call-done, f32[4,128]{1,0:T(4,128)S(1)} %get-tuple-element.90, f32[4,128]{1,0:T(4,128)S(1)} %get-tuple-element.104, f32[4,128]{1,0:T(4,128)S(1)} %get-tuple-element.103, f32[4,128]{1,0:T(4,128)S(1)} %get-tuple-element.102, ...), kind=kLoop, calls=%fused_computation.80 | loop fusion | flops 4194304 | bytes 2394128 | tf_op jit(solution)/shard_map/mul | solution.py:183
  256.1 0.8 multiply_reduce_fusion
  256.9 0.3 copy.178
  257.1 0.3 reshape.475
  257.4 0.1 rsqrt.21
  257.5 0.0 copy-done.3
  257.5 0.1 fusion.46
  257.7 3.7 %convolution_convert_fusion.1 = bf16[128,2048]{1,0:T(8,128)(2,1)S(1)} fusion(bf16[1024,2048]{0,1:T(8,128)(2,1)} %bitcast.378, bf16[128,512]{0,1:T(8,128)(2,1)S(1)} %fusion.46, bf16[128,512]{0,1:T(8,128)(2,1)S(1)} %fusion.47), kind=kOutput, calls=%fused_computation.4 | convolution fusion | flops 537657344 | bytes 4980736 | tf_op jit(solution)/shard_map/dot_general | solution.py:191
  261.4 9.1 %all_to_all.5 = bf16[2,64,2048]{2,1,0:T(8,128)(2,1)S(1)} all-to-all(bf16[2,64,2048]{2,1,0:T(8,128)(2,1)S(1)} %bitcast.380), channel_id=1, replica_groups=mesh['sp_0'=8,'sp_1'=8,'fs'=4,'tp'=2] {'tp'}, dimensions={0} | all-to-all | bytes 1048576 | tf_op jit(solution)/shard_map/all_to_all | solution.py:74
  270.5 0.8 reduce_sum.42
  (33 shorter events, 0.3 us)
Async XLA Ops:
  6.5 209.5 %copy-start = (bf16[2,256,256]{2,1,0:T(8,128)(2,1)S(1)}, bf16[2,256,256]{2,1,0:T(8,128)(2,1)}, u32[]{:S(2)}) copy-start(bf16[2,256,256]{2,1,0:T(8,128)(2,1)} %param.21) | copy-start | bytes 786436
  6.5 108.3 %all-gather.10.cloned.1.call-start = ((), (), s32[]{:S(2)}) async-start(), calls=%async_computation.1 | async-start | bytes 8519680 | tf_op jit(solution)/shard_map/all_gather | solution.py:113
  8.1 164.1 %all-gather.16.cloned.1.call-start = ((), (), s32[]{:S(2)}) async-start(), calls=%async_computation.4 | async-start | bytes 4718592 | tf_op jit(solution)/shard_map/all_gather | solution.py:23
  37.4 172.1 %all-gather.14.cloned.1.call-start = ((), (), s32[]{:S(2)}) async-start(), calls=%async_computation.3 | async-start | bytes 1179648 | tf_op jit(solution)/shard_map/all_gather | solution.py:52
  122.4 130.7 %all-gather.12.cloned.1.call-start = ((), (), s32[]{:S(2)}) async-start(), calls=%async_computation.2 | async-start | bytes 1179648 | tf_op jit(solution)/shard_map/all_gather | solution.py:52
  211.9 3.5 %collective-permute-start = (bf16[16,512]{1,0:T(8,128)(2,1)S(1)}, bf16[16,512]{1,0:T(8,128)(2,1)S(1)}, u32[]{:S(2)}, u32[]{:S(2)}) collective-permute-start(bf16[16,512]{1,0:T(8,128)(2,1)S(1)} %slice.306), channel_id=1, source_target_pairs={{0,8},{8,16},{16,24},{24,32},{32,40},{40,48},{48,56},{56,64},{64,7... | collective-permute-start | bytes 49160 | tf_op jit(solution)/shard_map/ppermute | solution.py:37
  216.0 0.7 copy-start.2
  216.0 37.1 %copy-start.1 = (bf16[32,128,128]{2,1,0:T(8,128)(2,1)S(1)}, bf16[32,128,128]{2,1,0:T(8,128)(2,1)}, u32[]{:S(2)}) copy-start(bf16[32,128,128]{2,1,0:T(8,128)(2,1)} %all-gather.14.cloned.1.call-done) | copy-start | bytes 3145732
  216.5 41.0 %copy-start.3 = (f32[512]{0:T(512)S(1)}, f32[512]{0:T(512)}, u32[]{:S(2)}) copy-start(f32[512]{0:T(512)} %param.25) | copy-start | bytes 6148
Sparse Core Ops, SparseCore 0:
  10.4 104.4 all-gather.9
  117.0 55.1 all-gather.15
  174.3 35.1 all-gather.13
  212.0 41.0 all-gather.11
where the time goes:
time: 279 us; the launch traced here: 278 us
  waiting for transfers between devices  159 us (57%)
  blocking collectives  69.3 us (25%)
  between operations  13.5 us (5%)
  other arithmetic  11.6 us (4%)
  matrix products  11.1 us (4%)
  local copies, waits for them, and re-layouts  10 us (4%)
  starting transfers between devices  2.81 us (1%)
    all_gather x1, waiting for transfers between devices, body(): lax.all_gather(stacked, SP, axis=0, tiled=True)  67.8 us
    all_gather x1, waiting for transfers between devices, all_blocks(): tiles = lax.all_gather(tiles, axes[k])  49.5 us
    all_gather x2, waiting for transfers between devices, carried_in(): lax.all_gather(part.astype(kind), axis)  42 us
    all_gather x1, blocking collectives, all_blocks(): tiles = lax.all_gather(tiles, axes[k])  27.3 us
    all_gather x2, blocking collectives, carried_in(): lax.all_gather(part.astype(kind), axis)  25.1 us
    all_to_all x1, blocking collectives, summed_on_arrival(): lax.all_to_all(tiles, axis, split_axis=0, concat_axis=0, tiled=True)  9.09 us
    all_gather x1, blocking collectives, body(): gathered = lax.all_gather(tokens, 'tp', axis=1, tiled=True)[0]  7.83 us
    transpose x1, local copies, waits for them, and re-layouts, all_blocks(): tiles = tiles.transpose(*back, *range(len(axes), tiles.ndim))  6.47 us
  transfers between devices with their start and end apart: 5, of which 4 were waited for; matrix products, arithmetic and copies ran while one was open for 7% of the time, Pallas kernels for 0%

commit v1 on v0

--- a/solution.py
+++ b/solution.py
@@ -109,9 +109,16 @@
         [pooling_input_weight, query_weight, forget_weight, value_weight], axis=1
     )
     out_local = jnp.concatenate([pooling_output_weight, recurrent_output_weight], axis=0)
-    projected = jnp.dot(
-        normed, lax.all_gather(stacked, SP, axis=0, tiled=True), preferred_element_type=jnp.float32
-    )
+    handle_indices = lambda local, group_axis: jnp.concatenate(
+        lax.all_to_all(
+            jnp.stack(lax.axis_size(group_axis) * [local], 0),
+            group_axis,
+            split_axis=0,
+            concat_axis=0,
+        ),
+        0,
+    )
+    projected = jnp.dot(normed, handle_indices(stacked, SP), preferred_element_type=jnp.float32)
     out_full = gathered_by_axis(out_local, SP, (0, 1), 1)
     rounded = lax.optimization_barrier(projected.astype(jnp.bfloat16))
     pool_input = rounded[:, :pool_width]

time: 279 us -> 452 us (1.62)
  blocking collectives: 69.3 us -> 289 us
  waiting for transfers between devices: 159 us -> 89.9 us
  starting transfers between devices: 2.81 us -> 20.6 us
    all_gather x1, blocking collectives: 27.3 us -> 236 us  [all_blocks(): tiles = lax.all_gather(tiles, axes[k])]
    all_gather x1 -> x0, waiting for transfers between devices: 67.8 us -> none  [body(): lax.all_gather(stacked, SP, axis=0, tiled=True)]
    all_to_all x0 -> x1, starting transfers between devices: none -> 17.5 us  [body(): lax.all_to_all(jnp.stack(lax.axis_size(group_axis) * [local], 0), group_a...]
    all_gather x2, blocking collectives: 25.1 us -> 31.9 us  [carried_in(): lax.all_gather(part.astype(kind), axis)]
  transfers between devices with their start and end apart: 5 -> 5, of which waited for: 4 -> 3; matrix products, arithmetic and copies ran while one was open for 7% -> 5% of each run, Pallas kernels for 0% -> 0%
where the time goes in v1:
time: 452 us
  blocking collectives  289 us (64%)
  waiting for transfers between devices  89.9 us (20%)
  starting transfers between devices  20.6 us (5%)
  local copies, waits for them, and re-layouts  14.3 us (3%)
  between operations  13.6 us (3%)
  other arithmetic  12.3 us (3%)
  matrix products  11.8 us (3%)
    all_gather x1, blocking collectives, all_blocks(): tiles = lax.all_gather(tiles, axes[k])  236 us
    all_gather x1, waiting for transfers between devices, all_blocks(): tiles = lax.all_gather(tiles, axes[k])  49.9 us
    all_gather x2, waiting for transfers between devices, carried_in(): lax.all_gather(part.astype(kind), axis)  39.9 us
    all_gather x2, blocking collectives, carried_in(): lax.all_gather(part.astype(kind), axis)  31.9 us
    all_to_all x1, starting transfers between devices, body(): lax.all_to_all(jnp.stack(lax.axis_size(group_axis) * [local], 0), group_a...  17.5 us
    all_gather x1, blocking collectives, body(): gathered = lax.all_gather(tokens, 'tp', axis=1, tiled=True)[0]  12 us
    all_to_all x1, blocking collectives, summed_on_arrival(): lax.all_to_all(tiles, axis, split_axis=0, concat_axis=0, tiled=True)  9.08 us
  transfers between devices with their start and end apart: 5, of which 3 were waited for; matrix products, arithmetic and copies ran while one was open for 5% of the time, Pallas kernels for 0%

profile of v1, /device:TPU:1, one launch (start us, length us, event | category | flops | bytes accessed | tf_op | source)
XLA Modules:
  0.0 451.7 jit_solution(7033305355287346072)
XLA Ops:
  6.5 0.9 pad_maximum_fusion
  7.4 4.3 stack.2
  11.7 0.0 copy-start.10
  11.7 0.0 copy-start.4
  11.7 17.5 %all-to-all-start = ((bf16[64,32,2048]{2,1,0:T(8,128)(2,1)}), bf16[64,32,2048]{2,1,0:T(8,128)(2,1)}, u32[]{:S(2)}, u32[]{:S(2)}) async-start(bf16[64,32,2048]{2,1,0:T(8,128)(2,1)} %stack.2), calls=%async_computation | async-start | bytes 16777216 | tf_op jit(solution)/shard_map/all_to_all | solution.py:113
  29.3 0.0 all-gather.13.cloned.1.call-start
  29.3 0.0 copy-done.5
  29.3 0.0 copy-done.6
  29.3 236.2 %all-gather.2 = bf16[8192,32]{0,1:T(8,128)(2,1)S(1)} all-gather(bf16[1024,32]{0,1:T(8,128)(2,1)S(1)} %pad_maximum_fusion.1), channel_id=4, replica_groups=mesh['sp_0'=8,'sp_1'=8,'fs'=4,'tp'=2] {'sp_0'}, dimensions={0}, use_global_device_ids=true | all-gather | bytes 589824 | tf_op jit(solution)/shard_map/all_gather | solution.py:23
  265.5 1.1 copy.197
  266.6 0.0 all-gather.13.cloned.1.call-update
  266.6 0.0 all-gather.11.cloned.1.call-start
  266.7 0.1 copy.177
  266.9 0.6 compare_convert_fusion.6
  267.5 0.6 compare_convert_fusion.8
  268.0 12.0 %all_gather.33 = bf16[1,128,2048]{2,1,0:T(8,128)(2,1)S(1)} all-gather(bf16[1,64,2048]{2,1,0:T(8,128)(2,1)S(1)} %copy-done.3), channel_id=1, replica_groups=mesh['sp_0'=8,'sp_1'=8,'fs'=4,'tp'=2] {'tp'}, dimensions={1}, use_global_device_ids=true | all-gather | bytes 786432 | tf_op jit(solution)/shard_map/all_gather | solution.py:103
  280.0 0.2 fusion.2
  280.2 0.0 all-to-all-done
  280.2 4.7 %convolution_convert_fusion = bf16[128,2048]{1,0:T(8,128)(2,1)S(1)} fusion(bf16[2048,2048]{1,0:T(8,128)(2,1)} %bitcast.1, bf16[1,128,2048]{2,1,0:T(8,128)(2,1)S(1)} %all_gather.33, f32[2048]{0:T(1024)S(1)} %copy-done.4, f32[128]{0:T(128)S(1)} %add_rsqrt_fusion.1), kind=kOutput, calls=%fused_computation.3 | convolution fusion | flops 1075052544 | bytes 9445888 | tf_op jit(solution)/shard_map/dot_general | solution.py:121
  284.9 0.2 negate_log-plus-one_fusion
  285.1 0.1 reshape.404
  285.2 0.1 reshape.403
  285.3 0.1 reshape.405
  285.4 0.7 fusion.89
  286.1 0.2 fusion.54
  286.4 0.2 exponential_multiply_fusion
  286.6 0.6 fusion.48
  287.2 0.0 copy-start.2
  287.2 0.5 while.13
  287.3 0.2 bitcast_add_fusion.2
  287.5 0.2 bitcast_add_fusion.2
  287.7 0.7 convert_element_type.535
  288.4 0.0 all-gather.11.cloned.1.call-update
  288.4 0.0 all-gather.9.cloned.1.call-start
  288.5 0.6 compare_convert_fusion.10
  289.1 0.6 compare_convert_fusion.12
  289.7 0.5 compare_convert_fusion.14
  290.2 0.1 minimum_convert_fusion
  290.3 49.9 %all-gather.13.cloned.1.call-done = bf16[64,1024,32]{1,0,2:T(8,128)(2,1)} async-done(((bf16[8,1024,32]{1,0,2:T(8,128)(2,1)}), bf16[64,1024,32]{1,0,2:T(8,128)(2,1)}) %all-gather.13.cloned.1.call-update) | async-done | bytes 4194320 | tf_op jit(solution)/shard_map/all_gather | solution.py:23
  340.2 6.4 %copy.176 = bf16[8,8,1024,32]{2,3,1,0:T(8,128)(2,1)} copy(bf16[8,8,1024,32]{2,0,1,3:T(8,128)(2,1)} %bitcast.376) | data formatting | bytes 8388608 | tf_op jit(solution)/shard_map/transpose | solution.py:26
  346.7 11.0 %all-gather.4 = bf16[8,4,128]{2,1,0:T(4,128)(2,1)S(1)} all-gather(bf16[1,4,128]{2,1,0:T(4,128)(2,1)S(1)} %fusion.75), channel_id=2, replica_groups=mesh['sp_0'=8,'sp_1'=8,'fs'=4,'tp'=2] {'sp_1'}, dimensions={0}, use_global_device_ids=true | all-gather | bytes 9216 | tf_op jit(solution)/shard_map/all_gather | solution.py:52
  357.7 20.9 %all_gather.35 = bf16[8,4,128]{2,1,0:T(4,128)(2,1)S(1)} all-gather(bf16[1,4,128]{2,1,0:T(4,128)(2,1)S(1)} %fusion.65), channel_id=1, replica_groups=mesh['sp_0'=8,'sp_1'=8,'fs'=4,'tp'=2] {'sp_0'}, dimensions={0}, use_global_device_ids=true | all-gather | bytes 9216 | tf_op jit(solution)/shard_map/all_gather | solution.py:52
  378.6 4.6 %all-gather.11.cloned.1.call-done = bf16[32,128,128]{2,1,0:T(8,128)(2,1)} async-done(((bf16[4,128,128]{2,1,0:T(8,128)(2,1)}), bf16[32,128,128]{2,1,0:T(8,128)(2,1)}) %all-gather.11.cloned.1.call-update) | async-done | bytes 1048592 | tf_op jit(solution)/shard_map/all_gather | solution.py:52
  383.2 2.4 fusion.52
  385.7 0.0 all-gather.9.cloned.1.call-update
  385.7 3.0 collective-permute-start
  388.7 0.5 convolution_multiply_fusion
  389.3 0.3 fusion.62
  389.5 0.0 collective-permute-done
  389.6 0.0 copy-start.8
  389.6 0.5 fusion.90
  390.1 1.2 convolution_bitcast_fusion
  391.3 0.1 copy.164
  391.5 0.1 fusion.47
  391.6 35.3 %all-gather.9.cloned.1.call-done = bf16[8,4,128,128]{3,2,1,0:T(8,128)(2,1)} async-done(((bf16[1,4,128,128]{3,2,1,0:T(8,128)(2,1)}), bf16[8,4,128,128]{3,2,1,0:T(8,128)(2,1)}) %all-gather.9.cloned.1.call-update) | async-done | bytes 1048592 | tf_op jit(solution)/shard_map/all_gather | solution.py:52
  426.9 2.9 fusion.44
  429.9 0.8 multiply_reduce_fusion
  430.7 0.3 copy.178
  430.9 0.3 reshape.494
  431.3 0.1 rsqrt.21
  431.3 0.1 fusion.46
  431.5 3.7 convolution_convert_fusion.1
  435.2 9.1 %all_to_all.10 = bf16[2,64,2048]{2,1,0:T(8,128)(2,1)S(1)} all-to-all(bf16[2,64,2048]{2,1,0:T(8,128)(2,1)S(1)} %bitcast.377), channel_id=1, replica_groups=mesh['sp_0'=8,'sp_1'=8,'fs'=4,'tp'=2] {'tp'}, dimensions={0} | all-to-all | bytes 1048576 | tf_op jit(solution)/shard_map/all_to_all | solution.py:74
  444.3 0.8 reduce_sum.42
  (45 shorter events, 0.3 us)
Async XLA Ops:
  6.5 383.6 %copy-start = (bf16[2,256,256]{2,1,0:T(8,128)(2,1)S(1)}, bf16[2,256,256]{2,1,0:T(8,128)(2,1)}, u32[]{:S(2)}) copy-start(bf16[2,256,256]{2,1,0:T(8,128)(2,1)} %param.21) | copy-start | bytes 786436
  11.7 17.6 %copy-start.5 = (bf16[512,32]{0,1:T(8,128)(2,1)S(1)}, bf16[512,32]{0,1:T(8,128)(2,1)}, u32[]{:S(2)}) copy-start(bf16[512,32]{0,1:T(8,128)(2,1)} %param.27) | copy-start | bytes 98308
  11.7 17.6 %copy-start.6 = (bf16[512,32]{0,1:T(8,128)(2,1)S(1)}, bf16[512,32]{0,1:T(8,128)(2,1)}, u32[]{:S(2)}) copy-start(bf16[512,32]{0,1:T(8,128)(2,1)} %param.26) | copy-start | bytes 98308
  11.7 255.0 %copy-start.9 = (f32[1,128,4]{1,2,0:T(4,128)S(1)}, f32[1,128,4]{1,2,0:T(4,128)}, u32[]{:S(2)}) copy-start(f32[1,128,4]{1,2,0:T(4,128)} %param.24) | copy-start | bytes 6148
  11.7 256.3 %copy-start.3 = (bf16[1,64,2048]{2,1,0:T(8,128)(2,1)S(1)}, bf16[1,64,2048]{2,1,0:T(8,128)(2,1)}, u32[]{:S(2)}) copy-start(bf16[1,64,2048]{2,1,0:T(8,128)(2,1)} %param.15) | copy-start | bytes 786436
  11.7 268.5 %copy-start.10 = (f32[512]{0:T(512)S(1)}, f32[512]{0:T(512)}, u32[]{:S(2)}) copy-start(f32[512]{0:T(512)} %param.23) | copy-start | bytes 6148
  11.7 268.5 %copy-start.4 = (f32[2048]{0:T(1024)S(1)}, f32[2048]{0:T(1024)}, u32[]{:S(2)}) copy-start(f32[2048]{0:T(1024)} %param.16) | copy-start | bytes 24580
  11.7 268.5 %all-to-all-start = ((bf16[64,32,2048]{2,1,0:T(8,128)(2,1)}), bf16[64,32,2048]{2,1,0:T(8,128)(2,1)}, u32[]{:S(2)}, u32[]{:S(2)}) async-start(bf16[64,32,2048]{2,1,0:T(8,128)(2,1)} %stack.2), calls=%async_computation | async-start | bytes 16777216 | tf_op jit(solution)/shard_map/all_to_all | solution.py:113
  29.3 311.0 %all-gather.13.cloned.1.call-start = ((), (), s32[]{:S(2)}) async-start(), calls=%async_computation.4 | async-start | bytes 4718592 | tf_op jit(solution)/shard_map/all_gather | solution.py:23
  266.6 116.6 %all-gather.11.cloned.1.call-start = ((), (), s32[]{:S(2)}) async-start(), calls=%async_computation.3 | async-start | bytes 1179648 | tf_op jit(solution)/shard_map/all_gather | solution.py:52
  287.2 102.3 %copy-start.2 = (bf16[128,512]{1,0:T(8,128)(2,1)S(1)}, bf16[128,512]{1,0:T(8,128)(2,1)}, u32[]{:S(2)}) copy-start(bf16[128,512]{1,0:T(8,128)(2,1)} %get-tuple-element.65) | copy-start | bytes 393220
  288.4 138.5 %all-gather.9.cloned.1.call-start = ((), (), s32[]{:S(2)}) async-start(), calls=%async_computation.2 | async-start | bytes 1179648 | tf_op jit(solution)/shard_map/all_gather | solution.py:52
  383.2 8.2 %copy-start.7 = (f32[512]{0:T(512)S(1)}, f32[512]{0:T(512)}, u32[]{:S(2)}) copy-start(f32[512]{0:T(512)} %param.22) | copy-start | bytes 6148
  385.7 41.3 %copy-start.1 = (bf16[32,128,128]{2,1,0:T(8,128)(2,1)S(1)}, bf16[32,128,128]{2,1,0:T(8,128)(2,1)}, u32[]{:S(2)}) copy-start(bf16[32,128,128]{2,1,0:T(8,128)(2,1)} %all-gather.11.cloned.1.call-done) | copy-start | bytes 3145732
  385.7 3.8 collective-permute-start
  389.6 41.8 %copy-start.8 = (f32[512]{0:T(512)S(1)}, f32[512]{0:T(512)}, u32[]{:S(2)}) copy-start(f32[512]{0:T(512)} %param.25) | copy-start | bytes 6148
Sparse Core Ops, SparseCore 0:
  266.7 73.4 all-gather.12
  342.3 40.9 all-gather.10
  385.8 41.0 all-gather.8
